TPU v7x, 512 devices: a whole 4x4x16 slice. The times are simulated.
512 devices in a mesh: ep: 128 (over z, x, core), tp: 4 (over y).
Axes of the slice: x: 4, y: 4, z: 16, core: 2. Of those that a mesh axis runs over, the one named last changes fastest.
Arguments:
- tokens: bfloat16 [1024, 1024], P('ep'), may hold values from -6 to 6
- lengths: int32 [1024], P('ep'), may hold values from 1 to 512, as said below
- cache_keys: bfloat16 [1024, 512, 4, 128], P('ep', None, 'tp'), may hold values from -2.5 to 2.5
- cache_values: bfloat16 [1024, 512, 4, 128], P('ep', None, 'tp'), may hold values from -6 to 6
- cache_cum: float32 [1024, 4, 512], P('ep', 'tp'), may hold values from -1536 to 0, as said below
- norm_gain: bfloat16 [1024], replicated, may hold values from 0.099609375 to 1.8984375
- query_weight: bfloat16 [1024, 1024], P(None, 'tp'), may hold values from -0.1875 to 0.1875
- key_weight: bfloat16 [1024, 512], P(None, 'tp'), may hold values from -0.1875 to 0.1875
- value_weight: bfloat16 [1024, 512], P(None, 'tp'), may hold values from -0.1875 to 0.1875
- forget_weight: bfloat16 [1024, 4], P(None, 'tp'), may hold values from -0.1875 to 0.1875
- forget_bias: float32 [4], P('tp'), may hold values from -1 to 2
- query_gain: bfloat16 [128], replicated, may hold values from 0.29882812 to 2.5
- key_gain: bfloat16 [128], replicated, may hold values from 0.099609375 to 1.8984375
- out_weight: bfloat16 [1024, 1024], P('tp'), may hold values from -0.1875 to 0.1875
- ffn_gain: bfloat16 [1024], replicated, may hold values from 0.099609375 to 1.8984375
- mix_weight: bfloat16 [1024], replicated, may hold values from -0.1875 to 0.1875
- shared_gate: bfloat16 [1024, 4096], P(None, 'ep'), may hold values from -0.1875 to 0.1875
- shared_up: bfloat16 [1024, 4096], P(None, 'ep'), may hold values from -0.1875 to 0.1875
- shared_down: bfloat16 [4096, 1024], P('ep', 'tp'), may hold values from -0.09375 to 0.09375
- routes: int32 [1024, 2], P('ep'), may hold values from 0 to 127, all different within a row; in each aligned block of 8 rows (0 to 7, 8 to 15, ...) at most 4 rows name the same one
- route_weights: float32 [1024, 2], P('ep'), may hold values from 0.1 to 1
- expert_gate: bfloat16 [128, 1024, 512], P('ep', None, 'tp'), may hold values from -0.1875 to 0.1875
- expert_up: bfloat16 [128, 1024, 512], P('ep', None, 'tp'), may hold values from -0.1875 to 0.1875
- expert_down: bfloat16 [128, 512, 1024], P('ep', 'tp'), may hold values from -0.25 to 0.25
Outputs:
- layer_out: bfloat16 [1024, 1024], P('ep', 'tp')
Inputs may be any that keep to these rules, and one draw needn't show every extreme that they name: `lengths`: at least one sequence has exactly 512 cached positions. `cache_cum`: along the positions each row never rises. `routes`: the 2 experts of a token differ; among the 8 rows of one device no expert is named by more than 4 rows, a bound that some block reaches.
All inputs are finite; a program needn't handle non-finite values.
Results may differ from a plain program's by a relative error of at most 0.013.
Values may be sent and summed in bfloat16 or wider, within the bound.
A program may use at most 64 MiB of HBM per device.

v0:
```python
import jax
import jax.numpy as jnp
from jax import lax
from jax.sharding import Mesh
from jax.sharding import PartitionSpec as P

CAP = 4
EP = ("ep_0", "ep_1", "ep_2")
epsilon = 1e-06


def copy_for_each(shard, axis):
    peers = lax.axis_size(axis)
    return lax.all_to_all(
        jnp.broadcast_to(shard[None], (peers, *shard.shape)), axis, 0, 0, tiled=True
    )


def of_everyone(shard, axis):
    return copy_for_each(shard, axis).astype(jnp.float32).sum(axis=0)


def cut_along(shard, dim, peers):
    before, after = (shard.shape[:dim], shard.shape[dim + 1 :])
    return jnp.moveaxis(shard.reshape(*before, peers, -1, *after), dim, 0)


def summed_on_arrival(shard, axis, dim):
    peers = lax.axis_size(axis)
    tiles = lax.all_to_all(cut_along(shard, dim, peers), axis, 0, 0, tiled=True)
    return jnp.sum(tiles.astype(jnp.float32), axis=0)


def sum_in_order(tiles, axes, sequence):
    shape = [lax.axis_size(a) for a in axes]
    tiles = tiles.reshape(*shape, *tiles.shape[1:])
    tiles = tiles.transpose(*sequence, *range(len(axes), tiles.ndim))
    tiles = tiles.reshape(-1, *tiles.shape[len(axes) :])
    for k in sequence:
        tiles = lax.psum_scatter(tiles, axes[k], scatter_dimension=0, tiled=True)
    return tiles[0]


def summed_rows(shard, axes, sequence, dim):
    peers = lax.axis_size(axes)
    return sum_in_order(cut_along(shard, dim, peers), axes, sequence)


def rms_norm(values, gain):
    values = values.astype(jnp.float32)
    return (
        values
        * lax.rsqrt(jnp.mean(values * values, axis=-1, keepdims=True) + epsilon)
        * gain.astype(jnp.float32)
    )


def per_device(
    tokens,
    lengths,
    cache_keys,
    cache_values,
    cache_cum,
    norm_gain,
    query_weight,
    key_weight,
    value_weight,
    forget_weight,
    forget_bias,
    query_gain,
    key_gain,
    out_weight,
    ffn_gain,
    mix_weight,
    shared_gate,
    shared_up,
    shared_down,
    routes,
    route_weights,
    expert_gate,
    expert_up,
    expert_down,
):
    seq_rows = tokens.shape[0]
    cache_len = cache_keys.shape[1]
    kv_local = cache_keys.shape[2]
    head_size = cache_keys.shape[3]
    normed = rms_norm(tokens, norm_gain).astype(jnp.bfloat16)
    query = jnp.dot(normed, query_weight, preferred_element_type=jnp.float32)
    query = rms_norm(query.reshape(seq_rows, kv_local, -1, head_size), query_gain).astype(
        jnp.bfloat16
    )
    new_key = jnp.dot(normed, key_weight, preferred_element_type=jnp.float32)
    new_key = rms_norm(new_key.reshape(seq_rows, kv_local, head_size), key_gain).astype(
        jnp.bfloat16
    )
    new_value = jnp.dot(normed, value_weight, preferred_element_type=jnp.float32).astype(
        jnp.bfloat16
    )
    new_value = new_value.reshape(seq_rows, kv_local, head_size)
    new_log = jax.nn.log_sigmoid(
        jnp.dot(normed, forget_weight, preferred_element_type=jnp.float32) + forget_bias
    )
    position = jnp.arange(cache_len, dtype=jnp.int32)
    live = position[None, :] < lengths[:, None]
    at_last = (position[None, :] == lengths[:, None] - 1)[:, None, :]
    last_cum = jnp.sum(jnp.where(at_last, cache_cum, 0.0), axis=-1)
    gate_bias = last_cum[:, :, None] - cache_cum + new_log[:, :, None]
    score_scale = head_size ** (-0.5)
    past = (
        jnp.einsum("skgd,spkd->skgp", query, cache_keys, preferred_element_type=jnp.float32)
        * score_scale
    )
    past = past + gate_bias[:, :, None, :]
    past = jnp.where(live[:, None, None, :], past, -jnp.inf)
    own = (
        jnp.sum(query.astype(jnp.float32) * new_key.astype(jnp.float32)[:, :, None, :], axis=-1)
        * score_scale
    )
    past_exp = jnp.exp(past)
    own_exp = jnp.exp(own)
    denominator = jnp.sum(past_exp, axis=-1) + own_exp
    past_prob = (past_exp / denominator[..., None]).astype(jnp.bfloat16)
    own_prob = (own_exp / denominator).astype(jnp.bfloat16)
    mixed = jnp.einsum(
        "skgp,spkd->skgd", past_prob, cache_values, preferred_element_type=jnp.float32
    )
    mixed = (
        mixed
        + own_prob.astype(jnp.float32)[..., None] * new_value.astype(jnp.float32)[:, :, None, :]
    )
    heads_out = mixed.astype(jnp.bfloat16).reshape(seq_rows, -1)
    partial_value = jnp.dot(heads_out, out_weight, preferred_element_type=jnp.float32)
    attended = of_everyone(partial_value.astype(jnp.bfloat16), "tp").astype(jnp.float32)
    residual = tokens.astype(jnp.float32) + attended
    ffn_in = rms_norm(residual, ffn_gain).astype(jnp.bfloat16)
    mix_gate = jax.nn.sigmoid(jnp.dot(ffn_in, mix_weight, preferred_element_type=jnp.float32))
    slice_width = ffn_in.shape[1] // lax.axis_size("tp")
    slice_start = lax.axis_index("tp") * slice_width
    ep_count = lax.axis_size(EP)
    local_experts = expert_gate.shape[0]
    num_experts = ep_count * local_experts
    topk = routes.shape[1]
    n_assign = seq_rows * topk
    order = jnp.arange(n_assign, dtype=jnp.int32)
    earlier = order[None, :] < order[:, None]
    slot_ids = jnp.arange(num_experts * CAP, dtype=jnp.int32)
    flat_route = routes.reshape(-1)
    same_expert = flat_route[:, None] == flat_route[None, :]
    slot_rank = jnp.sum(jnp.logical_and(same_expert, earlier), axis=1)
    slot_index = flat_route * CAP + slot_rank
    gathered_rows, gathered_routes = (
        lax.all_gather(ffn_in, EP, axis=0, tiled=True),
        lax.all_gather(routes, EP, axis=0, tiled=True),
    )
    pre_gate = jnp.dot(gathered_rows, shared_gate, preferred_element_type=jnp.float32)
    pre_up = jnp.dot(gathered_rows, shared_up, preferred_element_type=jnp.float32)
    shared_hidden = (jax.nn.silu(pre_gate) * pre_up).astype(jnp.bfloat16)
    terms = jnp.dot(shared_hidden, shared_down, preferred_element_type=jnp.float32)
    block_routes = gathered_routes.reshape(ep_count, n_assign)
    local_id = block_routes - lax.axis_index(EP) * local_experts
    mine = jnp.logical_and(local_id >= 0, local_id < local_experts)
    same_block = block_routes[:, :, None] == block_routes[:, None, :]
    block_rank = jnp.sum(jnp.logical_and(same_block, earlier[None, :, :]), axis=2)
    source = jnp.arange(ep_count, dtype=jnp.int32)[:, None]
    own_slot = source * (local_experts * CAP) + local_id * CAP + block_rank
    own_slot = jnp.where(mine, own_slot, -1).reshape(-1)
    pick_table = (own_slot[None, :] == slot_ids[:, None]).astype(jnp.bfloat16)
    repeated_all = jnp.repeat(gathered_rows, topk, axis=0)
    received = jnp.dot(pick_table, repeated_all, preferred_element_type=jnp.float32).astype(
        jnp.bfloat16
    )
    received = received.reshape(ep_count, local_experts, CAP, ffn_in.shape[1])
    pre_gate = jnp.einsum(
        "nekd,edf->nekf", received, expert_gate, preferred_element_type=jnp.float32
    )
    pre_up = jnp.einsum("nekd,edf->nekf", received, expert_up, preferred_element_type=jnp.float32)
    hidden = (jax.nn.silu(pre_gate) * pre_up).astype(jnp.bfloat16)
    part_out = jnp.einsum("nekf,efd->nekd", hidden, expert_down, preferred_element_type=jnp.float32)
    summed = summed_on_arrival(part_out.astype(jnp.bfloat16), "tp", 3)
    results = summed.astype(jnp.bfloat16)
    dense = summed_rows(terms, EP, (2, 0, 1), 0)
    returned = lax.all_to_all(results, EP, split_axis=0, concat_axis=0, tiled=True)
    returned = returned.reshape(num_experts * CAP, -1).astype(jnp.float32)
    norm_weights = route_weights / jnp.sum(route_weights, axis=1, keepdims=True)
    slot_table = slot_index.reshape(seq_rows, topk)
    combine = jnp.sum(
        (slot_table[:, :, None] == slot_ids[None, None, :]) * norm_weights[:, :, None], axis=1
    )
    routed = jnp.dot(combine, returned, precision=lax.Precision.HIGHEST)
    residual_slice = lax.dynamic_slice_in_dim(residual, slice_start, slice_width, 1)
    return (residual_slice + mix_gate[:, None] * dense + routed).astype(jnp.bfloat16)


def solution(mesh):
    finer = Mesh(mesh.devices.reshape(16, 4, 2, mesh.shape["tp"]), ("ep_0", "ep_1", "ep_2", "tp"))
    placed = (
        P(EP, None),
        P(EP),
        P(EP, None, "tp", None),
        P(EP, None, "tp", None),
        P(EP, "tp", None),
        P(),
        P(None, "tp"),
        P(None, "tp"),
        P(None, "tp"),
        P(None, "tp"),
        P("tp"),
        P(),
        P(),
        P("tp", None),
        P(),
        P(),
        P(None, EP),
        P(None, EP),
        P(EP, "tp"),
        P(EP, None),
        P(EP, None),
        P(EP, None, "tp"),
        P(EP, None, "tp"),
        P(EP, "tp", None),
    )
    return jax.shard_map(
        per_device, mesh=finer, in_specs=placed, out_specs=P(EP, "tp"), check_vma=False
    )
```

profile of v0, /device:TPU:8, one launch (start us, length us, event | category | flops | bytes accessed | tf_op | source)
XLA Modules:
  0.0 320.0 jit_solution(15933887718298431837)
XLA Ops:
  11.6 1.2 fusion.14
  12.7 1.3 multiply_reduce_fusion.2
  14.1 1.3 fusion.49
  20.2 9.0 %all-to-all-start = ((bf16[4,8,1024]{2,1,0:T(8,128)(2,1)}), bf16[4,8,1024]{2,1,0:T(8,128)(2,1)S(1)}, u32[]{:S(2)}, u32[]{:S(2)}) async-start(bf16[4,8,1024]{2,1,0:T(8,128)(2,1)} %broadcast_in_dim.26), calls=%async_computation | async-start | bytes 131072 | tf_op jit(solution)/shard_map/all_to_all | solution.py:14
  29.3 4.2 %all-to-all-done = bf16[4,8,1024]{2,1,0:T(8,128)(2,1)S(1)} async-done(((bf16[4,8,1024]{2,1,0:T(8,128)(2,1)}), bf16[4,8,1024]{2,1,0:T(8,128)(2,1)S(1)}, u32[]{:S(2)}, u32[]{:S(2)}) %all-to-all-start) | async-done | bytes 65568 | tf_op jit(solution)/shard_map/all_to_all | solution.py:14
  34.4 85.2 %all-gather = s32[128,8,2]{1,2,0:T(2,128)S(1)} all-gather(s32[1,8,2]{1,2,0:T(2,128)S(1)} %bitcast.132), channel_id=1, replica_groups=mesh['ep_0'=16,'ep_1'=4,'ep_2'=2,'tp'=4] {'ep_0','ep_1','ep_2'}, dimensions={0}, use_global_device_ids=true | all-gather | bytes 8256 | tf_op jit(solution)/shard_map/all_gather | solution.py:154
  119.9 54.6 %all-gather.3.cloned.1.call-done = bf16[1024,1024]{1,0:T(8,128)(2,1)} async-done(((bf16[8,1024]{1,0:T(8,128)(2,1)}), bf16[1024,1024]{1,0:T(8,128)(2,1)}) %all-gather.3.cloned.1.call-update) | async-done | bytes 2097168 | tf_op jit(solution)/shard_map/all_gather | solution.py:153
  174.5 2.5 fusion.72
  177.0 2.0 fusion.7
  179.0 2.4 copy.100
  182.5 1.0 copy.106
  183.5 1.3 mul.279
  184.8 3.6 %broadcast_in_dim.28 = bf16[1024,2,1024]{2,1,0:T(2,128)(2,1)} broadcast(bf16[1024,1024]{1,0:T(8,128)(2,1)S(1)} %copy-done.1), dimensions={0,2} | broadcast | bytes 6291456 | tf_op jit(solution)/shard_map/broadcast_in_dim | solution.py:169
  188.4 7.4 %reshape.353 = bf16[2048,1024]{1,0:T(8,128)(2,1)} reshape(bf16[1024,2,1024]{2,1,0:T(2,128)(2,1)} %broadcast_in_dim.28) | data formatting | bytes 8388608 | tf_op jit(solution)/shard_map/reshape | solution.py:169
  195.8 4.6 %fusion.2 = bf16[512,1024]{1,0:T(8,128)(2,1)S(1)} fusion(bf16[2048,1024]{1,0:T(8,128)(2,1)} %reshape.353, s32[2048]{0:T(1024)S(1)} %add_select_fusion), kind=kOutput, calls=%fused_computation.3 | convolution fusion | flops 2149056512 | bytes 5251072 | tf_op jit(solution)/shard_map/dot_general | solution.py:170
  200.9 2.3 convolution_bitcast_fusion.1
  203.2 2.3 convolution_convert_fusion
  205.5 1.1 copy.138
  206.6 5.0 %all-to-all-start.1 = ((bf16[4,128,1,4,256]{4,1,3,2,0:T(8,128)(2,1)}), bf16[4,128,1,4,256]{4,1,3,2,0:T(8,128)(2,1)S(1)}, u32[]{:S(2)}, u32[]{:S(2)}) async-start(bf16[4,128,1,4,256]{4,1,3,2,0:T(8,128)(2,1)} %bitcast.122), calls=%async_computation.4 | async-start | bytes 2097152 | tf_op jit(solution)/shard_map/all_to_all | solution.py:30
  212.3 13.3 %all-to-all-done.1 = bf16[4,128,1,4,256]{4,1,3,2,0:T(8,128)(2,1)S(1)} async-done(((bf16[4,128,1,4,256]{4,1,3,2,0:T(8,128)(2,1)}), bf16[4,128,1,4,256]{4,1,3,2,0:T(8,128)(2,1)S(1)}, u32[]{:S(2)}, u32[]{:S(2)}) %all-to-all-start.1) | async-done | bytes 1048608 | tf_op jit(solution)/shard_map/all_to_all | solution.py:30
  226.8 11.5 %all-to-all-start.2 = ((bf16[128,1,4,256]{3,2,1,0:T(4,128)(2,1)}), bf16[128,1,4,256]{3,2,1,0:T(4,128)(2,1)S(1)}, u32[]{:S(2)}, u32[]{:S(2)}) async-start(bf16[128,1,4,256]{3,2,1,0:T(4,128)(2,1)} %copy.113), calls=%async_computation.5 | async-start | bytes 524288 | tf_op jit(solution)/shard_map/all_to_all | solution.py:183
  238.9 44.9 %reduce-scatter.6.cloned.1.call-done = f32[4,8,256]{2,1,0:T(8,128)} async-done(((f32[64,8,256]{2,1,0:T(8,128)}), f32[4,8,256]{2,1,0:T(8,128)}) %reduce-scatter.6.cloned.1.call-update) | async-done | bytes 32784 | tf_op jit(solution)/shard_map/reduce_scatter | solution.py:40
  284.1 27.9 %reduce-scatter.8.cloned.1.call-done = f32[1,8,256]{2,1,0:T(8,128)} async-done(((f32[4,8,256]{2,1,0:T(8,128)}), f32[1,8,256]{2,1,0:T(8,128)}) %reduce-scatter.8.cloned.1.call-update) | async-done | bytes 8208 | tf_op jit(solution)/shard_map/reduce_scatter | solution.py:40
  312.0 1.5 fusion.12
  (92 shorter events, 14.5 us)
Async XLA Ops:
  6.5 12.0 %copy-start = (bf16[8,512,1,128]{3,1,2,0:T(8,128)(2,1)S(1)}, bf16[8,512,1,128]{3,1,2,0:T(8,128)(2,1)}, u32[]{:S(2)}) copy-start(bf16[8,512,1,128]{3,1,2,0:T(8,128)(2,1)} %param.26) | copy-start | bytes 3145732
  6.5 12.5 %copy-start.12 = (bf16[8,512,1,128]{3,1,2,0:T(8,128)(2,1)S(1)}, bf16[8,512,1,128]{3,1,2,0:T(8,128)(2,1)}, u32[]{:S(2)}) copy-start(bf16[8,512,1,128]{3,1,2,0:T(8,128)(2,1)} %param.27) | copy-start | bytes 3145732
  6.5 12.8 %copy-start.2 = (bf16[256,1024]{1,0:T(8,128)(2,1)S(1)}, bf16[256,1024]{1,0:T(8,128)(2,1)}, u32[]{:S(2)}) copy-start(bf16[256,1024]{1,0:T(8,128)(2,1)} %param.37) | copy-start | bytes 1572868
  12.7 16.5 %copy-start.10 = (bf16[1024]{0:T(1024)(128)(2,1)S(1)}, bf16[1024]{0:T(1024)(128)(2,1)}, u32[]{:S(2)}) copy-start(bf16[1024]{0:T(1024)(128)(2,1)} %param.38) | copy-start | bytes 6148
  12.7 20.7 %copy-start.3 = (bf16[8,1024]{1,0:T(8,128)(2,1)S(1)}, bf16[8,1024]{1,0:T(8,128)(2,1)}, u32[]{:S(2)}) copy-start(bf16[8,1024]{1,0:T(8,128)(2,1)} %param.24) | copy-start | bytes 49156
  14.1 20.3 %copy-start.8 = (s32[8,2]{0,1:T(2,128)S(1)}, s32[8,2]{0,1:T(2,128)}, u32[]{:S(2)}) copy-start(s32[8,2]{0,1:T(2,128)} %param.43) | copy-start | bytes 196
  15.4 159.1 %copy-start.4 = (bf16[1024,32]{0,1:T(8,128)(2,1)S(1)}, bf16[1024,32]{0,1:T(8,128)(2,1)}, u32[]{:S(2)}) copy-start(bf16[1024,32]{0,1:T(8,128)(2,1)} %param.40) | copy-start | bytes 196612
  19.4 157.6 %copy-start.5 = (bf16[1024,32]{0,1:T(8,128)(2,1)S(1)}, bf16[1024,32]{0,1:T(8,128)(2,1)}, u32[]{:S(2)}) copy-start(bf16[1024,32]{0,1:T(8,128)(2,1)} %param.41) | copy-start | bytes 196612
  19.4 157.6 %copy-start.7 = (bf16[32,256]{1,0:T(8,128)(2,1)S(1)}, bf16[32,256]{1,0:T(8,128)(2,1)}, u32[]{:S(2)}) copy-start(bf16[32,256]{1,0:T(8,128)(2,1)} %param.42) | copy-start | bytes 49156
  20.2 13.2 %all-to-all-start = ((bf16[4,8,1024]{2,1,0:T(8,128)(2,1)}), bf16[4,8,1024]{2,1,0:T(8,128)(2,1)S(1)}, u32[]{:S(2)}, u32[]{:S(2)}) async-start(bf16[4,8,1024]{2,1,0:T(8,128)(2,1)} %broadcast_in_dim.26), calls=%async_computation | async-start | bytes 131072 | tf_op jit(solution)/shard_map/all_to_all | solution.py:14
  29.3 145.2 %all-gather.3.cloned.1.call-start = ((), (), s32[]{:S(2)}) async-start(), calls=%async_computation.6 | async-start | bytes 2113536 | tf_op jit(solution)/shard_map/all_gather | solution.py:153
  34.3 177.3 %reduce-scatter.4.cloned.1.call-start = ((), (), s32[]{:S(2)}) async-start(), calls=%async_computation.7 | async-start | bytes 1572864 | tf_op jit(solution)/shard_map/reduce_scatter | solution.py:40
  174.5 2.5 copy-start.1
  206.6 32.2 %copy-start.11 = (bf16[1024]{0:T(1024)(128)(2,1)S(1)}, bf16[1024]{0:T(1024)(128)(2,1)}, u32[]{:S(2)}) copy-start(bf16[1024]{0:T(1024)(128)(2,1)} %param.39) | copy-start | bytes 6148
  206.6 32.2 %copy-start.9 = (f32[8,2]{0,1:T(2,128)S(1)}, f32[8,2]{0,1:T(2,128)}, u32[]{:S(2)}) copy-start(f32[8,2]{0,1:T(2,128)} %param.44) | copy-start | bytes 196
  206.6 77.2 %copy-start.6 = (bf16[8,1024]{1,0:T(8,128)(2,1)S(1)}, bf16[8,1024]{1,0:T(8,128)(2,1)}, u32[]{:S(2)}) copy-start(bf16[8,1024]{1,0:T(8,128)(2,1)} %multiply_convert_fusion) | copy-start | bytes 49156
  206.6 19.0 %all-to-all-start.1 = ((bf16[4,128,1,4,256]{4,1,3,2,0:T(8,128)(2,1)}), bf16[4,128,1,4,256]{4,1,3,2,0:T(8,128)(2,1)S(1)}, u32[]{:S(2)}, u32[]{:S(2)}) async-start(bf16[4,128,1,4,256]{4,1,3,2,0:T(8,128)(2,1)} %bitcast.122), calls=%async_computation.4 | async-start | bytes 2097152 | tf_op jit(solution)/shard_map/all_to_all | solution.py:30
  211.6 72.2 %reduce-scatter.6.cloned.1.call-start = ((), (), s32[]{:S(2)}) async-start(), calls=%async_computation.8 | async-start | bytes 557056 | tf_op jit(solution)/shard_map/reduce_scatter | solution.py:40
  226.8 57.2 %all-to-all-start.2 = ((bf16[128,1,4,256]{3,2,1,0:T(4,128)(2,1)}), bf16[128,1,4,256]{3,2,1,0:T(4,128)(2,1)S(1)}, u32[]{:S(2)}, u32[]{:S(2)}) async-start(bf16[128,1,4,256]{3,2,1,0:T(4,128)(2,1)} %copy.113), calls=%async_computation.5 | async-start | bytes 524288 | tf_op jit(solution)/shard_map/all_to_all | solution.py:183
  238.2 73.8 %reduce-scatter.8.cloned.1.call-start = ((), (), s32[]{:S(2)}) async-start(), calls=%async_computation.9 | async-start | bytes 40960 | tf_op jit(solution)/shard_map/reduce_scatter | solution.py:40
Sparse Core Ops, SparseCore 0:
  34.4 140.0 all-gather.2
  181.6 15.1 reduce-scatter.3
  215.2 68.5 reduce-scatter.5
  286.4 25.4 reduce-scatter.7
where the time goes:
time: 321 us; the launch traced here: 320 us
  waiting for transfers between devices  146 us (45%)
  blocking collectives  85.2 us (27%)
  starting transfers between devices  25.5 us (8%)
  matrix products  21.1 us (7%)
  local copies, waits for them, and re-layouts  20.6 us (6%)
  between operations  14 us (4%)
  other arithmetic  7.9 us (2%)
    all_gather x1, blocking collectives, per_device(): lax.all_gather(routes, EP, axis=0, tiled=True)  85.2 us
    reduce_scatter x3, waiting for transfers between devices, sum_in_order(): tiles = lax.psum_scatter(tiles, axes[k], scatter_dimension=0, tiled=True)  72.8 us
    all_gather x1, waiting for transfers between devices, per_device(): lax.all_gather(ffn_in, EP, axis=0, tiled=True)  54.6 us
    all_to_all x1, waiting for transfers between devices, summed_on_arrival(): tiles = lax.all_to_all(cut_along(shard, dim, peers), axis, 0, 0, tiled=True)  13.3 us
    all_to_all x1, starting transfers between devices, per_device(): lax.all_to_all(results, EP, split_axis=0, concat_axis=0, tiled=True)  11.5 us
    all_to_all x1, starting transfers between devices, copy_for_each(): lax.all_to_all(jnp.broadcast_to(shard[None], (peers, *shard.shape)), axis...  9.04 us
    reshape x1, local copies, waits for them, and re-layouts, per_device(): repeated_all = jnp.repeat(gathered_rows, topk, axis=0)  7.4 us
  transfers between devices with their start and end apart: 7, of which 5 were waited for; matrix products, arithmetic and copies ran while one was open for 9% of the time, Pallas kernels for 0%

commit v1 on v0

--- a/solution.py
+++ b/solution.py
@@ -150,7 +150,7 @@
     slot_rank = jnp.sum(jnp.logical_and(same_expert, earlier), axis=1)
     slot_index = flat_route * CAP + slot_rank
     gathered_rows, gathered_routes = (
-        lax.all_gather(ffn_in, EP, axis=0, tiled=True),
+        jnp.concatenate(lax.all_to_all(jnp.stack([ffn_in] * lax.axis_size(EP)), EP, 0, 0), axis=0),
         lax.all_gather(routes, EP, axis=0, tiled=True),
     )
     pre_gate = jnp.dot(gathered_rows, shared_gate, preferred_element_type=jnp.float32)

time: 321 us -> 367 us (1.14)
  blocking collectives: 85.2 us -> 167 us
  waiting for transfers between devices: 146 us -> 91.5 us
  starting transfers between devices: 25.5 us -> 44.5 us
    all_gather x1, blocking collectives: 85.2 us -> 167 us  [per_device(): lax.all_gather(routes, EP, axis=0, tiled=True)]
    all_gather x1 -> x0, waiting for transfers between devices: 54.6 us -> none  [per_device(): lax.all_gather(ffn_in, EP, axis=0, tiled=True)]
    all_to_all x0 -> x1, starting transfers between devices: none -> 15.8 us  [per_device(): lax.all_to_all(jnp.stack([ffn_in] * lax.axis_size(EP)), EP, 0, 0)]
  transfers between devices with their start and end apart: 7 -> 7, of which waited for: 5 -> 4; matrix products, arithmetic and copies ran while one was open for 9% -> 7% of each run, Pallas kernels for 0% -> 0%
where the time goes in v1:
time: 367 us; the launch traced here: 365 us
  blocking collectives  167 us (46%)
  waiting for transfers between devices  91.5 us (25%)
  starting transfers between devices  44.5 us (12%)
  local copies, waits for them, and re-layouts  22 us (6%)
  matrix products  19.4 us (5%)
  between operations  14 us (4%)
  other arithmetic  7.3 us (2%)
    all_gather x1, blocking collectives, per_device(): lax.all_gather(routes, EP, axis=0, tiled=True)  167 us
    reduce_scatter x3, waiting for transfers between devices, sum_in_order(): tiles = lax.psum_scatter(tiles, axes[k], scatter_dimension=0, tiled=True)  72.9 us
    all_to_all x1, starting transfers between devices, per_device(): lax.all_to_all(jnp.stack([ffn_in] * lax.axis_size(EP)), EP, 0, 0)  15.8 us
    all_to_all x1, starting transfers between devices, per_device(): lax.all_to_all(results, EP, split_axis=0, concat_axis=0, tiled=True)  14.4 us
    all_to_all x1, waiting for transfers between devices, summed_on_arrival(): tiles = lax.all_to_all(cut_along(shard, dim, peers), axis, 0, 0, tiled=True)  13.6 us
    all_to_all x1, starting transfers between devices, copy_for_each(): lax.all_to_all(jnp.broadcast_to(shard[None], (peers, *shard.shape)), axis...  9.04 us
  transfers between devices with their start and end apart: 7, of which 4 were waited for; matrix products, arithmetic and copies ran while one was open for 7% of the time, Pallas kernels for 0%

profile of v1, /device:TPU:8, one launch (start us, length us, event | category | flops | bytes accessed | tf_op | source)
XLA Modules:
  0.0 365.3 jit_solution(11416481461757201476)
XLA Ops:
  11.6 1.2 fusion.14
  12.7 1.3 multiply_reduce_fusion.2
  14.1 1.4 fusion.49
  20.2 9.0 %all-to-all-start = ((bf16[4,8,1024]{2,1,0:T(8,128)(2,1)}), bf16[4,8,1024]{2,1,0:T(8,128)(2,1)S(1)}, u32[]{:S(2)}, u32[]{:S(2)}) async-start(bf16[4,8,1024]{2,1,0:T(8,128)(2,1)} %broadcast_in_dim.26), calls=%async_computation | async-start | bytes 131072 | tf_op jit(solution)/shard_map/all_to_all | solution.py:14
  29.3 4.2 %all-to-all-done = bf16[4,8,1024]{2,1,0:T(8,128)(2,1)S(1)} async-done(((bf16[4,8,1024]{2,1,0:T(8,128)(2,1)}), bf16[4,8,1024]{2,1,0:T(8,128)(2,1)S(1)}, u32[]{:S(2)}, u32[]{:S(2)}) %all-to-all-start) | async-done | bytes 65568 | tf_op jit(solution)/shard_map/all_to_all | solution.py:14
  33.7 1.6 stack.2
  35.3 15.8 %all-to-all-start.1 = ((bf16[128,8,1024]{2,1,0:T(8,128)(2,1)}), bf16[128,8,1024]{2,1,0:T(8,128)(2,1)S(1)}, u32[]{:S(2)}, u32[]{:S(2)}) async-start(bf16[128,8,1024]{2,1,0:T(8,128)(2,1)} %stack.2), calls=%async_computation.1 | async-start | bytes 4194304 | tf_op jit(solution)/shard_map/all_to_all | solution.py:153
  51.2 166.7 %all-gather = s32[128,8,2]{1,2,0:T(2,128)S(1)} all-gather(s32[1,8,2]{1,2,0:T(2,128)S(1)} %bitcast.137), channel_id=1, replica_groups=mesh['ep_0'=16,'ep_1'=4,'ep_2'=2,'tp'=4] {'ep_0','ep_1','ep_2'}, dimensions={0}, use_global_device_ids=true | all-gather | bytes 8256 | tf_op jit(solution)/shard_map/all_gather | solution.py:154
  218.9 2.0 fusion.7
  220.9 2.4 copy.100
  224.4 1.0 copy.106
  225.5 1.3 mul.279
  226.8 3.6 broadcast_in_dim.28
  230.3 7.2 %reshape.359 = bf16[2048,1024]{1,0:T(8,128)(2,1)} reshape(bf16[1024,2,1024]{2,1,0:T(2,128)(2,1)} %broadcast_in_dim.28) | data formatting | bytes 8388608 | tf_op jit(solution)/shard_map/reshape | solution.py:169
  237.6 4.6 %fusion.2 = bf16[512,1024]{1,0:T(8,128)(2,1)S(1)} fusion(bf16[2048,1024]{1,0:T(8,128)(2,1)} %reshape.359, s32[2048]{0:T(1024)S(1)} %add_select_fusion), kind=kOutput, calls=%fused_computation.3 | convolution fusion | flops 2149056512 | bytes 5251072 | tf_op jit(solution)/shard_map/dot_general | solution.py:170
  242.6 2.3 convolution_bitcast_fusion.1
  244.9 2.3 convolution_convert_fusion
  247.3 1.1 copy.138
  248.4 5.1 %all-to-all-start.2 = ((bf16[4,128,1,4,256]{4,1,3,2,0:T(8,128)(2,1)}), bf16[4,128,1,4,256]{4,1,3,2,0:T(8,128)(2,1)S(1)}, u32[]{:S(2)}, u32[]{:S(2)}) async-start(bf16[4,128,1,4,256]{4,1,3,2,0:T(8,128)(2,1)} %bitcast.126), calls=%async_computation.5 | async-start | bytes 2097152 | tf_op jit(solution)/shard_map/all_to_all | solution.py:30
  254.2 13.6 %all-to-all-done.2 = bf16[4,128,1,4,256]{4,1,3,2,0:T(8,128)(2,1)S(1)} async-done(((bf16[4,128,1,4,256]{4,1,3,2,0:T(8,128)(2,1)}), bf16[4,128,1,4,256]{4,1,3,2,0:T(8,128)(2,1)S(1)}, u32[]{:S(2)}, u32[]{:S(2)}) %all-to-all-start.2) | async-done | bytes 1048608 | tf_op jit(solution)/shard_map/all_to_all | solution.py:30
  269.0 14.4 %all-to-all-start.3 = ((bf16[128,1,4,256]{3,2,1,0:T(4,128)(2,1)}), bf16[128,1,4,256]{3,2,1,0:T(4,128)(2,1)S(1)}, u32[]{:S(2)}, u32[]{:S(2)}) async-start(bf16[128,1,4,256]{3,2,1,0:T(4,128)(2,1)} %copy.113), calls=%async_computation.6 | async-start | bytes 524288 | tf_op jit(solution)/shard_map/all_to_all | solution.py:183
  284.1 44.3 %reduce-scatter.6.cloned.1.call-done = f32[4,8,256]{2,1,0:T(8,128)} async-done(((f32[64,8,256]{2,1,0:T(8,128)}), f32[4,8,256]{2,1,0:T(8,128)}) %reduce-scatter.6.cloned.1.call-update) | async-done | bytes 32784 | tf_op jit(solution)/shard_map/reduce_scatter | solution.py:40
  328.7 28.6 %reduce-scatter.8.cloned.1.call-done = f32[1,8,256]{2,1,0:T(8,128)} async-done(((f32[4,8,256]{2,1,0:T(8,128)}), f32[1,8,256]{2,1,0:T(8,128)}) %reduce-scatter.8.cloned.1.call-update) | async-done | bytes 8208 | tf_op jit(solution)/shard_map/reduce_scatter | solution.py:40
  357.3 1.5 fusion.12
  (88 shorter events, 14.6 us)
Async XLA Ops:
  6.5 12.0 %copy-start = (bf16[8,512,1,128]{3,1,2,0:T(8,128)(2,1)S(1)}, bf16[8,512,1,128]{3,1,2,0:T(8,128)(2,1)}, u32[]{:S(2)}) copy-start(bf16[8,512,1,128]{3,1,2,0:T(8,128)(2,1)} %param.26) | copy-start | bytes 3145732
  6.5 12.5 %copy-start.10 = (bf16[8,512,1,128]{3,1,2,0:T(8,128)(2,1)S(1)}, bf16[8,512,1,128]{3,1,2,0:T(8,128)(2,1)}, u32[]{:S(2)}) copy-start(bf16[8,512,1,128]{3,1,2,0:T(8,128)(2,1)} %param.27) | copy-start | bytes 3145732
  6.5 12.8 %copy-start.1 = (bf16[256,1024]{1,0:T(8,128)(2,1)S(1)}, bf16[256,1024]{1,0:T(8,128)(2,1)}, u32[]{:S(2)}) copy-start(bf16[256,1024]{1,0:T(8,128)(2,1)} %param.37) | copy-start | bytes 1572868
  12.7 16.5 %copy-start.8 = (bf16[1024]{0:T(1024)(128)(2,1)S(1)}, bf16[1024]{0:T(1024)(128)(2,1)}, u32[]{:S(2)}) copy-start(bf16[1024]{0:T(1024)(128)(2,1)} %param.38) | copy-start | bytes 6148
  12.7 20.7 %copy-start.2 = (bf16[8,1024]{1,0:T(8,128)(2,1)S(1)}, bf16[8,1024]{1,0:T(8,128)(2,1)}, u32[]{:S(2)}) copy-start(bf16[8,1024]{1,0:T(8,128)(2,1)} %param.24) | copy-start | bytes 49156
  20.2 13.2 %all-to-all-start = ((bf16[4,8,1024]{2,1,0:T(8,128)(2,1)}), bf16[4,8,1024]{2,1,0:T(8,128)(2,1)S(1)}, u32[]{:S(2)}, u32[]{:S(2)}) async-start(bf16[4,8,1024]{2,1,0:T(8,128)(2,1)} %broadcast_in_dim.26), calls=%async_computation | async-start | bytes 131072 | tf_op jit(solution)/shard_map/all_to_all | solution.py:14
  35.3 15.9 %copy-start.6 = (s32[8,2]{0,1:T(2,128)S(1)}, s32[8,2]{0,1:T(2,128)}, u32[]{:S(2)}) copy-start(s32[8,2]{0,1:T(2,128)} %param.43) | copy-start | bytes 196
  35.3 182.9 %copy-start.3 = (bf16[1024,32]{0,1:T(8,128)(2,1)S(1)}, bf16[1024,32]{0,1:T(8,128)(2,1)}, u32[]{:S(2)}) copy-start(bf16[1024,32]{0,1:T(8,128)(2,1)} %param.40) | copy-start | bytes 196612
  35.3 182.8 %all-to-all-start.1 = ((bf16[128,8,1024]{2,1,0:T(8,128)(2,1)}), bf16[128,8,1024]{2,1,0:T(8,128)(2,1)S(1)}, u32[]{:S(2)}, u32[]{:S(2)}) async-start(bf16[128,8,1024]{2,1,0:T(8,128)(2,1)} %stack.2), calls=%async_computation.1 | async-start | bytes 4194304 | tf_op jit(solution)/shard_map/all_to_all | solution.py:153
  51.1 167.8 %copy-start.4 = (bf16[1024,32]{0,1:T(8,128)(2,1)S(1)}, bf16[1024,32]{0,1:T(8,128)(2,1)}, u32[]{:S(2)}) copy-start(bf16[1024,32]{0,1:T(8,128)(2,1)} %param.41) | copy-start | bytes 196612
  51.1 167.8 %copy-start.5 = (bf16[32,256]{1,0:T(8,128)(2,1)S(1)}, bf16[32,256]{1,0:T(8,128)(2,1)}, u32[]{:S(2)}) copy-start(bf16[32,256]{1,0:T(8,128)(2,1)} %param.42) | copy-start | bytes 49156
  51.1 202.4 %reduce-scatter.4.cloned.1.call-start = ((), (), s32[]{:S(2)}) async-start(), calls=%async_computation.7 | async-start | bytes 1572864 | tf_op jit(solution)/shard_map/reduce_scatter | solution.py:40
  248.4 35.6 %copy-start.9 = (bf16[1024]{0:T(1024)(128)(2,1)S(1)}, bf16[1024]{0:T(1024)(128)(2,1)}, u32[]{:S(2)}) copy-start(bf16[1024]{0:T(1024)(128)(2,1)} %param.39) | copy-start | bytes 6148
  248.4 35.7 %copy-start.7 = (f32[8,2]{0,1:T(2,128)S(1)}, f32[8,2]{0,1:T(2,128)}, u32[]{:S(2)}) copy-start(f32[8,2]{0,1:T(2,128)} %param.44) | copy-start | bytes 196
  248.4 19.5 %all-to-all-start.2 = ((bf16[4,128,1,4,256]{4,1,3,2,0:T(8,128)(2,1)}), bf16[4,128,1,4,256]{4,1,3,2,0:T(8,128)(2,1)S(1)}, u32[]{:S(2)}, u32[]{:S(2)}) async-start(bf16[4,128,1,4,256]{4,1,3,2,0:T(8,128)(2,1)} %bitcast.126), calls=%async_computation.5 | async-start | bytes 2097152 | tf_op jit(solution)/shard_map/all_to_all | solution.py:30
  253.5 75.0 %reduce-scatter.6.cloned.1.call-start = ((), (), s32[]{:S(2)}) async-start(), calls=%async_computation.8 | async-start | bytes 557056 | tf_op jit(solution)/shard_map/reduce_scatter | solution.py:40
  269.0 59.6 %all-to-all-start.3 = ((bf16[128,1,4,256]{3,2,1,0:T(4,128)(2,1)}), bf16[128,1,4,256]{3,2,1,0:T(4,128)(2,1)S(1)}, u32[]{:S(2)}, u32[]{:S(2)}) async-start(bf16[128,1,4,256]{3,2,1,0:T(4,128)(2,1)} %copy.113), calls=%async_computation.6 | async-start | bytes 524288 | tf_op jit(solution)/shard_map/all_to_all | solution.py:183
  283.4 73.9 %reduce-scatter.8.cloned.1.call-start = ((), (), s32[]{:S(2)}) async-start(), calls=%async_computation.9 | async-start | bytes 40960 | tf_op jit(solution)/shard_map/reduce_scatter | solution.py:40
Sparse Core Ops, SparseCore 0:
  223.5 16.6 reduce-scatter.3
  257.1 71.3 reduce-scatter.5
  331.3 25.9 reduce-scatter.7
